TPU v7x, 32 devices: a whole 2x2x4 slice. The times are simulated.
32 devices in a mesh: ep: 16 (over z, y, x), tp: 2 (over core).
Axes of the slice: x: 2, y: 2, z: 4, core: 2. Of those that a mesh axis runs over, the one named last changes fastest.
Arguments:
- tokens: bfloat16 [512, 2048], P('ep'), may hold values from -6 to 6
- lru_state: float32 [512, 1024], P('ep', 'tp'), may hold values from -6 to 6
- conv_window: bfloat16 [512, 3, 1024], P('ep', None, 'tp'), may hold values from -6 to 6
- gain_mix_in: float32 [2048], replicated, may hold values from 0.1 to 1.9
- gain_mix_out: float32 [2048], replicated, may hold values from 0.1 to 1.9
- gain_ffn_in: float32 [2048], replicated, may hold values from 0.1 to 1.9
- gain_ffn_out: float32 [2048], replicated, may hold values from 0.1 to 1.9
- w_branch: bfloat16 [2048, 1024], P(None, 'tp'), may hold values from -0.125 to 0.125
- w_input: bfloat16 [2048, 1024], P(None, 'tp'), may hold values from -0.125 to 0.125
- conv_taps: bfloat16 [4, 1024], P(None, 'tp'), may hold values from -3 to 3
- gate_a: bfloat16 [8, 128, 128], P('tp'), may hold values from -0.5 to 0.5
- gate_x: bfloat16 [8, 128, 128], P('tp'), may hold values from -0.5 to 0.5
- decay_rate: float32 [1024], P('tp'), may hold values from 0.001 to 0.3
- w_mix_out: bfloat16 [1024, 2048], P('tp'), may hold values from -0.1875 to 0.1875
- routes: int32 [512, 4], P('ep'), may hold values from 0 to 15, all different within a row; in each aligned block of 32 rows (0 to 31, 32 to 63, ...) at most 16 rows name the same one
- route_weight: float32 [512, 4], P('ep'), may hold values from 0.2 to 1.5
- expert_gate: bfloat16 [16, 2048, 512], P('ep', None, 'tp'), may hold values from -0.125 to 0.125
- expert_up: bfloat16 [16, 2048, 512], P('ep', None, 'tp'), may hold values from -0.125 to 0.125
- expert_down: bfloat16 [16, 512, 2048], P('ep', 'tp'), may hold values from -0.25 to 0.25
- shared_gate: bfloat16 [2048, 512], P(None, 'tp'), may hold values from -0.125 to 0.125
- shared_up: bfloat16 [2048, 512], P(None, 'tp'), may hold values from -0.125 to 0.125
- shared_down: bfloat16 [512, 2048], P('tp'), may hold values from -0.25 to 0.25
Outputs:
- layer_out: bfloat16 [512, 2048], P('ep')
- new_state: float32 [512, 1024], P('ep', 'tp')
- new_window: bfloat16 [512, 3, 1024], P('ep', None, 'tp')
Inputs may be any that keep to these rules, and one draw needn't show every extreme that they name: `routes`: each row names 4 different experts. Within the rows of one device (aligned blocks of 32 rows) no expert is named by more than 16 entries, a bound that some block reaches.
All inputs are finite; a program needn't handle non-finite values.
Results may differ from a plain program's by a relative error of at most 0.014.
Values may be sent and summed in bfloat16 or wider, within the bound.
A program may use at most 64 MiB of HBM per device.

v0:
```python
import jax
import jax.numpy as jnp
from jax import lax
from jax.sharding import PartitionSpec as P


def rms_norm(value, gain):
    return value * lax.rsqrt(jnp.mean(value * value, axis=-1, keepdims=True) + 1e-06) * gain


def rounded_term(value):
    return lax.optimization_barrier(value.astype(jnp.bfloat16)).astype(jnp.float32)


def on_device(
    tokens,
    lru_state,
    conv_window,
    gain_mix_in,
    gain_mix_out,
    gain_ffn_in,
    gain_ffn_out,
    w_branch,
    w_input,
    conv_taps,
    gate_a,
    gate_x,
    decay_rate,
    w_mix_out,
    routes,
    route_weight,
    expert_gate,
    expert_up,
    expert_down,
    shared_gate,
    shared_up,
    shared_down,
):
    resid = tokens.astype(jnp.float32)
    normed = rms_norm(resid, gain_mix_in).astype(jnp.bfloat16)
    branch = jnp.dot(normed, w_branch, preferred_element_type=jnp.float32)
    inflow = jnp.dot(normed, w_input, preferred_element_type=jnp.float32).astype(jnp.bfloat16)
    window = jnp.concatenate([conv_window, inflow[:, None, :]], axis=1)
    new_window = window[:, 1:]
    conv = jnp.sum(window.astype(jnp.float32) * conv_taps.astype(jnp.float32)[None], axis=1)
    count, local_ch = conv.shape
    groups, group_dim = (gate_a.shape[0], gate_a.shape[1])
    grouped = conv.astype(jnp.bfloat16).reshape(count, groups, group_dim)
    recur_gate = jax.nn.sigmoid(
        jnp.einsum("sbi,bij->sbj", grouped, gate_a, preferred_element_type=jnp.float32).reshape(
            count, local_ch
        )
    )
    input_gate = jax.nn.sigmoid(
        jnp.einsum("sbi,bij->sbj", grouped, gate_x, preferred_element_type=jnp.float32).reshape(
            count, local_ch
        )
    )
    log_decay = -8.0 * recur_gate * decay_rate[None]
    new_state = (
        jnp.exp(log_decay) * lru_state + jnp.sqrt(-jnp.expm1(2.0 * log_decay)) * conv * input_gate
    )
    gated = (new_state * jax.nn.gelu(branch)).astype(jnp.bfloat16)
    mix_term = rounded_term(jnp.dot(gated, w_mix_out, preferred_element_type=jnp.float32))
    mixed = lax.psum(mix_term.astype(jnp.bfloat16), "tp").astype(jnp.float32)
    middle = (resid + rms_norm(mixed, gain_mix_out)).astype(jnp.bfloat16)
    ffn_in = rms_norm(middle.astype(jnp.float32), gain_ffn_in).astype(jnp.bfloat16)
    width = ffn_in.shape[1]
    top = routes.shape[1]
    local_exp = expert_gate.shape[0]
    experts = local_exp * lax.axis_size("ep")
    capacity = max(2, 2 * count * top // experts)
    flat = routes.reshape(count * top)
    onehot = (flat[:, None] == jnp.arange(experts, dtype=jnp.int32)[None, :]).astype(jnp.int32)
    rank = jnp.sum(onehot * (jnp.cumsum(onehot, axis=0) - 1), axis=-1)
    dest = flat * capacity + rank
    slot_ids = jnp.arange(experts * capacity, dtype=jnp.int32)
    placed = jnp.any(dest.reshape(count, top)[None, :, :] == slot_ids[:, None, None], axis=-1)
    outbound = jnp.dot(placed.astype(jnp.bfloat16), ffn_in, preferred_element_type=jnp.float32)
    outbound = outbound.astype(jnp.bfloat16).reshape(experts, capacity, width)
    shared_hidden = (
        jax.nn.silu(jnp.dot(ffn_in, shared_gate, preferred_element_type=jnp.float32))
        * jnp.dot(ffn_in, shared_up, preferred_element_type=jnp.float32)
    ).astype(jnp.bfloat16)
    shared = lax.psum(
        rounded_term(
            jnp.dot(shared_hidden, shared_down, preferred_element_type=jnp.float32)
        ).astype(jnp.bfloat16),
        "tp",
    ).astype(jnp.float32)
    share = width // lax.axis_size("tp")
    own = lax.dynamic_slice_in_dim(outbound, lax.axis_index("tp") * share, share, 2)
    arrived = lax.all_to_all(own, "ep", split_axis=0, concat_axis=1, tiled=True)
    rows = lax.all_gather(arrived, "tp", axis=2, tiled=True)
    hidden = (
        jax.nn.silu(
            jnp.einsum("erd,edf->erf", rows, expert_gate, preferred_element_type=jnp.float32)
        )
        * jnp.einsum("erd,edf->erf", rows, expert_up, preferred_element_type=jnp.float32)
    ).astype(jnp.bfloat16)
    summed = lax.psum_scatter(
        rounded_term(
            jnp.einsum("erf,efd->erd", hidden, expert_down, preferred_element_type=jnp.float32)
        ).astype(jnp.bfloat16),
        "tp",
        scatter_dimension=2,
        tiled=True,
    )
    back = lax.all_to_all(summed, "ep", split_axis=1, concat_axis=0, tiled=True)
    flat_out = back.reshape(experts * capacity, share)
    picked = flat_out[dest].reshape(count, top, flat_out.shape[1])
    routed_share = jnp.sum(picked.astype(jnp.float32) * route_weight[:, :, None], axis=1).astype(
        jnp.bfloat16
    )
    routed = lax.all_gather(routed_share, "tp", axis=1, tiled=True)
    total = routed.astype(jnp.float32) + shared
    layer_out = (middle.astype(jnp.float32) + rms_norm(total, gain_ffn_out)).astype(jnp.bfloat16)
    return (layer_out, new_state, new_window)


def solution(mesh):
    placed = (
        P("ep", None),
        P("ep", "tp"),
        P("ep", None, "tp"),
        P(),
        P(),
        P(),
        P(),
        P(None, "tp"),
        P(None, "tp"),
        P(None, "tp"),
        P("tp", None, None),
        P("tp", None, None),
        P("tp"),
        P("tp", None),
        P("ep", None),
        P("ep", None),
        P("ep", None, "tp"),
        P("ep", None, "tp"),
        P("ep", "tp", None),
        P(None, "tp"),
        P(None, "tp"),
        P("tp", None),
    )
    return jax.shard_map(
        on_device,
        mesh=mesh,
        in_specs=placed,
        out_specs=(P("ep", None), P("ep", "tp"), P("ep", None, "tp")),
        check_vma=False,
    )
```

profile of v0, /device:TPU:0, one launch (start us, length us, event | category | flops | bytes accessed | tf_op | source)
XLA Modules:
  0.0 134.1 jit_solution(11292914418998984690)
XLA Ops:
  7.2 0.0 copy-start
  7.2 0.0 copy-start.2
  7.2 0.0 copy-start.10
  7.2 0.0 copy-start.3
  7.3 0.0 all-reduce.3.cloned.1.call-start
  7.3 1.2 fusion.24
  8.5 0.7 convert_element_type.92
  9.2 2.2 %fusion.10 = bf16[32,1,512]{2,0,1:T(8,128)(2,1)S(1)} fusion(bf16[2048,512]{1,0:T(8,128)(2,1)} %param.30, bf16[32,2048]{1,0:T(8,128)(2,1)} %param.22, f32[2048]{0:T(1024)} %param.25, f32[32]{0:T(128)S(1)} %add_rsqrt_fusion.3), kind=kOutput, calls=%fused_computation.19 | convolution fusion | flops 67387392 | bytes 2269312 | tf_op jit(solution)/shard_map/dot_general | solution.py:42
  11.4 0.0 copy-start.5
  11.5 0.2 fusion.5
  11.6 0.2 fusion.9
  11.9 0.1 fusion.49
  12.0 0.0 copy-start.7
  12.0 0.0 copy-start.13
  12.0 0.0 copy-start.12
  12.0 0.0 copy-start.8
  12.0 3.2 %convolution_convert_fusion.3 = bf16[32,2048]{1,0:T(8,128)(2,1)} fusion(bf16[512,2048]{1,0:T(8,128)(2,1)S(1)} %copy-done, f32[32,512]{1,0:T(8,128)S(1)} %fusion.49, bf16[2048,512]{1,0:T(8,128)(2,1)} %param.29, bf16[32,2048]{1,0:T(8,128)(2,1)S(1)} %copy-done.2, f32[2048]{0:T(1024)S(1)} %copy-done.10, f32[32]{0:T(128)S(1)} %add_rsqrt_fusion.3), kind=kOutput, calls=%fused_computation.5 | convolution fusion | flops 134709248 | bytes 4530304 | tf_op jit(solution)/shard_map/dot_general | solution.py:64
  15.3 0.0 all-reduce.3.cloned.1.call-update
  15.3 0.0 all-gather.2.cloned.1.call-start
  15.3 0.1 copy.57
  15.4 0.1 eq.28
  15.5 0.1 fusion.50
  15.6 0.2 reduce_window_sum.11
  15.8 0.2 select_reduce_fusion
  16.0 0.1 reduce_sum.71
  16.1 0.6 broadcast_multiply_fusion
  16.7 0.1 copy.59
  16.8 0.1 fusion.38
  16.9 19.2 %all-reduce.3.cloned.1.call-done = bf16[32,2048]{1,0:T(8,128)(2,1)} async-done(((bf16[32,2048]{1,0:T(8,128)(2,1)}), bf16[32,2048]{1,0:T(8,128)(2,1)}) %all-reduce.3.cloned.1.call-update) | async-done | bytes 131088 | tf_op jit(solution)/shard_map/psum | solution.py:65
  36.1 1.0 fusion.22
  37.1 1.1 fusion.28
  38.3 0.5 convolution_convert_fusion.1
  38.9 22.2 %all_to_all.21 = bf16[16,16,1024]{2,1,0:T(8,128)(2,1)} all-to-all(bf16[16,16,1024]{2,1,0:T(8,128)(2,1)S(1)} %constant_dynamic-slice_fusion), channel_id=1, replica_groups=mesh['ep'=16,'tp'=2] {'ep'}, dimensions={0} | all-to-all | bytes 1048576 | tf_op jit(solution)/shard_map/all_to_all | solution.py:93
  61.1 0.0 all-gather.2.cloned.1.call-update
  61.1 0.0 reduce-scatter.2.cloned.1.call-start
  61.1 7.5 %all-gather.2.cloned.1.call-done = bf16[1,256,2048]{2,1,0:T(8,128)(2,1)} async-done(((bf16[1,256,1024]{2,1,0:T(8,128)(2,1)}), bf16[1,256,2048]{2,1,0:T(8,128)(2,1)}) %all-gather.2.cloned.1.call-update) | async-done | bytes 1048592 | tf_op jit(solution)/shard_map/all_gather | solution.py:94
  68.6 2.1 %fusion.14 = f32[256,256]{1,0:T(8,128)S(1)} fusion(bf16[1,2048,256]{2,1,0:T(8,128)(2,1)} %param.38, bf16[1,256,2048]{2,1,0:T(8,128)(2,1)} %all-gather.2.cloned.1.call-done), kind=kOutput, calls=%fused_computation.24 | convolution fusion | flops 268435456 | bytes 2359296 | tf_op jit(solution)/shard_map/erd,edf->erf/dot_general | solution.py:97
  70.7 3.8 %fusion = bf16[1,256,2048]{2,1,0:T(8,128)(2,1)} fusion(bf16[1,256,2048]{2,1,0:T(8,128)(2,1)} %param.40, bf16[1,2048,256]{2,1,0:T(8,128)(2,1)} %param.39, bf16[1,256,2048]{2,1,0:T(8,128)(2,1)S(1)} %copy-done.1, f32[256,256]{1,0:T(8,128)S(1)} %fusion.14), kind=kOutput, calls=%fused_computation.3 | convolution fusion | flops 537788416 | bytes 4456448 | tf_op jit(solution)/shard_map/erf,efd->erd/dot_general | solution.py:103
  74.5 0.0 reduce-scatter.2.cloned.1.call-update
  74.6 0.8 mul.225
  75.4 0.8 copy.61
  76.2 8.1 %reduce-scatter.2.cloned.1.call-done = bf16[1,256,1024]{2,1,0:T(8,128)(2,1)} async-done(((bf16[1,256,2048]{2,1,0:T(8,128)(2,1)}), bf16[1,256,1024]{2,1,0:T(8,128)(2,1)}) %reduce-scatter.2.cloned.1.call-update) | async-done | bytes 524304 | tf_op jit(solution)/shard_map/reduce_scatter | solution.py:101
  84.3 1.9 %copy.81 = bf16[1,256,1024]{2,0,1:T(2,128)(2,1)S(1)} copy(bf16[1,256,1024]{2,1,0:T(8,128)(2,1)} %reduce-scatter.2.cloned.1.call-done) | data formatting | bytes 1048576 | tf_op jit(solution)/shard_map/reduce_scatter | solution.py:101
  86.1 0.0 copy-start.4
  86.2 0.5 broadcast.143
  86.7 4.5 %reduce = bf16[256,1024]{1,0:T(8,128)(2,1)} reduce(bf16[256,1,1024]{2,1,0:T(2,128)(2,1)S(1)} %bitcast.73, bf16[]{:T(256)} %broadcast.143), dimensions={1}, to_apply=%bitcast.70.reduce_sub_computation | reduce | bytes 1048578
  91.2 2.2 %reshape.155 = bf16[16,2,8192]{2,1,0:T(2,128)(2,1)} reshape(bf16[256,1024]{1,0:T(8,128)(2,1)} %reduce) | data formatting | bytes 1048576
  93.4 6.8 %all-to-all-start.1 = ((bf16[16,2,8192]{2,1,0:T(2,128)(2,1)}), bf16[16,2,8192]{2,1,0:T(2,128)(2,1)S(1)}, u32[]{:S(2)}, u32[]{:S(2)}) async-start(bf16[16,2,8192]{2,1,0:T(2,128)(2,1)} %reshape.155), calls=%async_computation.2 | async-start | bytes 1048576 | tf_op jit(solution)/shard_map/all_to_all | solution.py:109
  100.2 0.0 all-reduce.5.cloned.1.call-start
  100.3 0.7 fusion.39
  100.9 1.5 %fusion.82 = f32[32,256]{1,0:T(8,128)S(1)} fusion(bf16[2048,256]{1,0:T(8,128)(2,1)} %param.41, bf16[32,2048]{1,0:T(8,128)(2,1)S(1)} %get-tuple-element.4, f32[2048]{0:T(1024)S(1)} %copy-done.8, f32[32]{0:T(128)S(1)} %add_rsqrt_fusion.1), kind=kOutput, calls=%fused_computation.113 | convolution fusion | flops 33816576 | bytes 1220736 | tf_op jit(solution)/shard_map/dot_general | solution.py:82
  102.5 3.0 %convolution_convert_fusion.2 = bf16[32,2048]{1,0:T(8,128)(2,1)} fusion(bf16[256,2048]{1,0:T(8,128)(2,1)} %param.43, bf16[2048,256]{1,0:T(8,128)(2,1)} %param.42, f32[32,256]{1,0:T(8,128)S(1)} %fusion.82, bf16[32,2048]{1,0:T(8,128)(2,1)S(1)} %get-tuple-element.4, f32[2048]{0:T(1024)S(1)} %copy-done.8, f32[32]{0:T(128)S(1)} %add_rsqrt_fusion.1), kind=kOutput, calls=%fused_computation.4 | convolution fusion | flops 67485696 | bytes 2400384 | tf_op jit(solution)/shard_map/dot_general | solution.py:87
  105.5 0.0 all-reduce.5.cloned.1.call-update
  105.5 10.2 %all-to-all-done.1 = bf16[16,2,8192]{2,1,0:T(2,128)(2,1)S(1)} async-done(((bf16[16,2,8192]{2,1,0:T(2,128)(2,1)}), bf16[16,2,8192]{2,1,0:T(2,128)(2,1)S(1)}, u32[]{:S(2)}, u32[]{:S(2)}) %all-to-all-start.1) | async-done | bytes 524320 | tf_op jit(solution)/shard_map/all_to_all | solution.py:109
  115.7 1.8 %reshape.156 = bf16[256,1,1024]{2,1,0:T(2,128)(2,1)} reshape(bf16[16,2,8192]{2,1,0:T(2,128)(2,1)S(1)} %all-to-all-done.1) | data formatting | bytes 1048576
  117.4 1.4 %copy.80 = bf16[1,256,1024]{2,1,0:T(8,128)(2,1)S(1)} copy(bf16[1,256,1024]{2,0,1:T(2,128)(2,1)} %bitcast.72) | data formatting | bytes 1048576
  118.8 0.0 copy-start.11
  118.9 0.9 gather_fusion
  119.7 0.2 reshape.146
  119.9 0.4 multiply_reduce_fusion
  120.3 1.9 %all_gather.7 = bf16[32,2048]{1,0:T(8,128)(2,1)S(1)} all-gather(bf16[32,1024]{1,0:T(8,128)(2,1)S(1)} %multiply_reduce_fusion), channel_id=1, replica_groups=mesh['ep'=16,'tp'=2] {'tp'}, dimensions={1}, use_global_device_ids=true | all-gather | bytes 196608 | tf_op jit(solution)/shard_map/all_gather | solution.py:115
  122.2 2.7 %all-reduce.5.cloned.1.call-done = bf16[32,2048]{1,0:T(8,128)(2,1)} async-done(((bf16[32,2048]{1,0:T(8,128)(2,1)}), bf16[32,2048]{1,0:T(8,128)(2,1)}) %all-reduce.5.cloned.1.call-update) | async-done | bytes 131088 | tf_op jit(solution)/shard_map/psum | solution.py:85
  124.8 1.1 multiply_reduce_fusion.1
  125.9 1.7 %fusion.31 = bf16[32,2048]{1,0:T(8,128)(2,1)} fusion(bf16[32,2048]{1,0:T(8,128)(2,1)S(1)} %get-tuple-element.4, bf16[32,2048]{1,0:T(8,128)(2,1)} %all-reduce.5.cloned.1.call-done, bf16[32,2048]{1,0:T(8,128)(2,1)S(1)} %all_gather.7, f32[2048]{0:T(1024)S(1)} %copy-done.11, f32[32]{0:T(128)S(1)} %add_rsqrt_fusion), kind=kLoop, calls=%fused_computation.47 | loop fusion | flops 524288 | bytes 532608 | tf_op jit(solution)/shard_map/convert_element_type | solution.py:117
  (32 shorter events, 0.2 us)
Async XLA Ops:
  7.2 4.8 %copy-start = (bf16[512,2048]{1,0:T(8,128)(2,1)S(1)}, bf16[512,2048]{1,0:T(8,128)(2,1)}, u32[]{:S(2)}) copy-start(bf16[512,2048]{1,0:T(8,128)(2,1)} %param.35) | copy-start | bytes 6291460
  7.2 4.8 %copy-start.2 = (bf16[32,2048]{1,0:T(8,128)(2,1)S(1)}, bf16[32,2048]{1,0:T(8,128)(2,1)}, u32[]{:S(2)}) copy-start(bf16[32,2048]{1,0:T(8,128)(2,1)} %param.22) | copy-start | bytes 393220
  7.2 4.8 %copy-start.10 = (f32[2048]{0:T(1024)S(1)}, f32[2048]{0:T(1024)}, u32[]{:S(2)}) copy-start(f32[2048]{0:T(1024)} %param.25) | copy-start | bytes 24580
  7.2 4.2 %copy-start.3 = (bf16[32,3,512]{2,0,1:T(8,128)(2,1)S(1)}, bf16[32,3,512]{2,0,1:T(8,128)(2,1)}, u32[]{:S(2)}) copy-start(bf16[32,3,512]{2,0,1:T(8,128)(2,1)} %param.24) | copy-start | bytes 294916
  7.2 4.2 %copy-start.15 = (bf16[4,128,128]{2,1,0:T(8,128)(2,1)S(1)}, bf16[4,128,128]{2,1,0:T(8,128)(2,1)}, u32[]{:S(2)}) copy-start(bf16[4,128,128]{2,1,0:T(8,128)(2,1)} %param.33) | copy-start | bytes 393220
  7.2 4.4 %copy-start.16 = (bf16[4,128,128]{2,1,0:T(8,128)(2,1)S(1)}, bf16[4,128,128]{2,1,0:T(8,128)(2,1)}, u32[]{:S(2)}) copy-start(bf16[4,128,128]{2,1,0:T(8,128)(2,1)} %param.32) | copy-start | bytes 393220
  7.2 4.6 %copy-start.14 = (f32[512]{0:T(512)S(1)}, f32[512]{0:T(512)}, u32[]{:S(2)}) copy-start(f32[512]{0:T(512)} %param.34) | copy-start | bytes 6148
  7.2 4.6 %copy-start.9 = (f32[32,512]{1,0:T(8,128)S(1)}, f32[32,512]{1,0:T(8,128)}, u32[]{:S(2)}) copy-start(f32[32,512]{1,0:T(8,128)} %param.23) | copy-start | bytes 196612
  7.3 28.8 %all-reduce.3.cloned.1.call-start = ((), (), s32[]{:S(2)}) async-start(), calls=%async_computation.3 | async-start | bytes 262144 | tf_op jit(solution)/shard_map/psum | solution.py:65
  11.4 3.8 %copy-start.5 = (bf16[32,1,512]{2,0,1:T(8,128)(2,1)}, bf16[32,1,512]{2,0,1:T(8,128)(2,1)S(1)}, u32[]{:S(2)}) copy-start(bf16[32,1,512]{2,0,1:T(8,128)(2,1)S(1)} %fusion.10) | copy-start | bytes 98308
  12.0 3.3 %copy-start.7 = (f32[32,512]{1,0:T(8,128)}, f32[32,512]{1,0:T(8,128)S(1)}, u32[]{:S(2)}) copy-start(f32[32,512]{1,0:T(8,128)S(1)} %fusion.49) | copy-start | bytes 196612
  12.0 3.4 %copy-start.13 = (s32[32,4]{0,1:T(4,128)S(1)}, s32[32,4]{0,1:T(4,128)}, u32[]{:S(2)}) copy-start(s32[32,4]{0,1:T(4,128)} %param.36) | copy-start | bytes 1540
  12.0 25.1 %copy-start.12 = (f32[2048]{0:T(1024)S(1)}, f32[2048]{0:T(1024)}, u32[]{:S(2)}) copy-start(f32[2048]{0:T(1024)} %param.26) | copy-start | bytes 24580
  12.0 26.3 %copy-start.8 = (f32[2048]{0:T(1024)S(1)}, f32[2048]{0:T(1024)}, u32[]{:S(2)}) copy-start(f32[2048]{0:T(1024)} %param.27) | copy-start | bytes 24580
  15.3 53.4 %all-gather.2.cloned.1.call-start = ((), (), s32[]{:S(2)}) async-start(), calls=%async_computation.4 | async-start | bytes 1572864 | tf_op jit(solution)/shard_map/all_gather | solution.py:94
  61.1 23.2 %reduce-scatter.2.cloned.1.call-start = ((), (), s32[]{:S(2)}) async-start(), calls=%async_computation.5 | async-start | bytes 1572864 | tf_op jit(solution)/shard_map/reduce_scatter | solution.py:101
  68.6 2.1 %copy-start.1 = (bf16[1,256,2048]{2,1,0:T(8,128)(2,1)S(1)}, bf16[1,256,2048]{2,1,0:T(8,128)(2,1)}, u32[]{:S(2)}) copy-start(bf16[1,256,2048]{2,1,0:T(8,128)(2,1)} %all-gather.2.cloned.1.call-done) | copy-start | bytes 3145732
  86.1 14.1 %copy-start.4 = (bf16[32,3,512]{2,0,1:T(8,128)(2,1)S(1)}, bf16[32,3,512]{2,0,1:T(8,128)(2,1)}, u32[]{:S(2)}) copy-start(bf16[32,3,512]{2,0,1:T(8,128)(2,1)} %param.24) | copy-start | bytes 294916
  86.2 14.1 %copy-start.6 = (bf16[32,1,512]{2,0,1:T(8,128)(2,1)S(1)}, bf16[32,1,512]{2,0,1:T(8,128)(2,1)}, u32[]{:S(2)}) copy-start(bf16[32,1,512]{2,0,1:T(8,128)(2,1)} %copy-done.5) | copy-start | bytes 98308
  93.4 22.3 %all-to-all-start.1 = ((bf16[16,2,8192]{2,1,0:T(2,128)(2,1)}), bf16[16,2,8192]{2,1,0:T(2,128)(2,1)S(1)}, u32[]{:S(2)}, u32[]{:S(2)}) async-start(bf16[16,2,8192]{2,1,0:T(2,128)(2,1)} %reshape.155), calls=%async_computation.2 | async-start | bytes 1048576 | tf_op jit(solution)/shard_map/all_to_all | solution.py:109
  100.2 24.7 %all-reduce.5.cloned.1.call-start = ((), (), s32[]{:S(2)}) async-start(), calls=%async_computation.6 | async-start | bytes 262144 | tf_op jit(solution)/shard_map/psum | solution.py:85
  118.8 7.1 %copy-start.11 = (f32[2048]{0:T(1024)S(1)}, f32[2048]{0:T(1024)}, u32[]{:S(2)}) copy-start(f32[2048]{0:T(1024)} %param.28) | copy-start | bytes 24580
Sparse Core Ops, SparseCore 0:
  15.4 20.6 all-reduce.2
  61.2 7.3 all-gather.1
  74.7 9.5 reduce-scatter.1
  105.6 19.1 all-reduce.4
where the time goes:
time: 135 us; the launch traced here: 134 us
  waiting for transfers between devices  47.7 us (35%)
  blocking collectives  24.1 us (18%)
  matrix products  16.7 us (12%)
  between operations  14.2 us (11%)
  other arithmetic  13.6 us (10%)
  local copies, waits for them, and re-layouts  10.9 us (8%)
  starting transfers between devices  6.93 us (5%)
    all_to_all x1, blocking collectives, on_device(): arrived = lax.all_to_all(own, 'ep', split_axis=0, concat_axis=1, tiled=True)  22.2 us
    psum x1, waiting for transfers between devices, on_device(): mixed = lax.psum(mix_term.astype(jnp.bfloat16), 'tp').astype(jnp.float32)  19.2 us
    all_to_all x1, waiting for transfers between devices, on_device(): back = lax.all_to_all(summed, 'ep', split_axis=1, concat_axis=0, tiled=True)  10.2 us
    reduce_scatter x1, waiting for transfers between devices, on_device(): lax.psum_scatter(rounded_term(jnp.einsum('erf,efd->erd', hidden, expert_d...  8.14 us
    all_gather x1, waiting for transfers between devices, on_device(): rows = lax.all_gather(arrived, 'tp', axis=2, tiled=True)  7.49 us
    unnamed x40, local copies, waits for them, and re-layouts  6.86 us
    all_to_all x1, starting transfers between devices, on_device(): back = lax.all_to_all(summed, 'ep', split_axis=1, concat_axis=0, tiled=True)  6.77 us
    unnamed x1, other arithmetic  4.5 us
  transfers between devices with their start and end apart: 5, of which 5 were waited for; matrix products, arithmetic and copies ran while one was open for 10% of the time, Pallas kernels for 0%

commit v1 on v0

--- a/solution.py
+++ b/solution.py
@@ -106,7 +106,10 @@
         scatter_dimension=2,
         tiled=True,
     )
-    back = lax.all_to_all(summed, "ep", split_axis=1, concat_axis=0, tiled=True)
+    back = jnp.concatenate(
+        lax.all_to_all(jnp.stack(jnp.split(summed, lax.axis_size("ep"), axis=1)), "ep", 0, 0),
+        axis=0,
+    )
     flat_out = back.reshape(experts * capacity, share)
     picked = flat_out[dest].reshape(count, top, flat_out.shape[1])
     routed_share = jnp.sum(picked.astype(jnp.float32) * route_weight[:, :, None], axis=1).astype(

time: 135 us -> 149 us (1.10)
  local copies, waits for them, and re-layouts: 10.9 us -> 24.9 us
  other arithmetic: 13.6 us -> 9.12 us
  waiting for transfers between devices: 47.7 us -> 50.9 us
    unnamed x40 -> x51, local copies, waits for them, and re-layouts: 6.86 us -> 21.4 us
    unnamed x1 -> x0, other arithmetic: 4.5 us -> none
    psum x1, waiting for transfers between devices: 2.65 us -> 5.84 us  [on_device(): lax.psum(rounded_term(jnp.dot(shared_hidden, shared_down, preferred_eleme...]
    reduce_scatter x1 -> x0, local copies, waits for them, and re-layouts: 1.85 us -> none  [on_device(): lax.psum_scatter(rounded_term(jnp.einsum('erf,efd->erd', hidden, expert_d...]
  transfers between devices with their start and end apart: 5 -> 5, of which waited for: 5 -> 5; matrix products, arithmetic and copies ran while one was open for 10% -> 7% of each run, Pallas kernels for 0% -> 0%
where the time goes in v1:
time: 149 us; the launch traced here: 147 us
  waiting for transfers between devices  50.9 us (34%)
  local copies, waits for them, and re-layouts  24.9 us (17%)
  blocking collectives  24.1 us (16%)
  matrix products  16.7 us (11%)
  between operations  14.1 us (9%)
  other arithmetic  9.12 us (6%)
  starting transfers between devices  6.93 us (5%)
    all_to_all x1, blocking collectives, on_device(): arrived = lax.all_to_all(own, 'ep', split_axis=0, concat_axis=1, tiled=True)  22.2 us
    unnamed x51, local copies, waits for them, and re-layouts  21.4 us
    psum x1, waiting for transfers between devices, on_device(): mixed = lax.psum(mix_term.astype(jnp.bfloat16), 'tp').astype(jnp.float32)  19.2 us
    all_to_all x1, waiting for transfers between devices, on_device(): lax.all_to_all(jnp.stack(jnp.split(summed, lax.axis_size('ep'), axis=1)),...  10.2 us
    reduce_scatter x1, waiting for transfers between devices, on_device(): lax.psum_scatter(rounded_term(jnp.einsum('erf,efd->erd', hidden, expert_d...  8.11 us
    all_gather x1, waiting for transfers between devices, on_device(): rows = lax.all_gather(arrived, 'tp', axis=2, tiled=True)  7.49 us
    all_to_all x1, starting transfers between devices, on_device(): lax.all_to_all(jnp.stack(jnp.split(summed, lax.axis_size('ep'), axis=1)),...  6.77 us
    psum x1, waiting for transfers between devices, on_device(): lax.psum(rounded_term(jnp.dot(shared_hidden, shared_down, preferred_eleme...  5.84 us
  transfers between devices with their start and end apart: 5, of which 5 were waited for; matrix products, arithmetic and copies ran while one was open for 7% of the time, Pallas kernels for 0%

profile of v1, /device:TPU:0, one launch (start us, length us, event | category | flops | bytes accessed | tf_op | source)
XLA Modules:
  0.0 146.8 jit_solution(12892355222082966497)
XLA Ops:
  7.2 0.0 copy-start
  7.3 0.0 all-reduce.3.cloned.1.call-start
  7.3 1.2 fusion.24
  8.5 0.7 convert_element_type.92
  9.2 2.2 %fusion.10 = bf16[32,1,512]{2,0,1:T(8,128)(2,1)S(1)} fusion(bf16[2048,512]{1,0:T(8,128)(2,1)} %param.30, bf16[32,2048]{1,0:T(8,128)(2,1)} %param.22, f32[2048]{0:T(1024)} %param.25, f32[32]{0:T(128)S(1)} %add_rsqrt_fusion.3), kind=kOutput, calls=%fused_computation.19 | convolution fusion | flops 67387392 | bytes 2269312 | tf_op jit(solution)/shard_map/dot_general | solution.py:42
  11.5 0.2 fusion.5
  11.6 0.2 fusion.9
  11.9 0.1 fusion.49
  12.0 3.2 %convolution_convert_fusion.3 = bf16[32,2048]{1,0:T(8,128)(2,1)} fusion(bf16[512,2048]{1,0:T(8,128)(2,1)S(1)} %copy-done, f32[32,512]{1,0:T(8,128)S(1)} %fusion.49, bf16[2048,512]{1,0:T(8,128)(2,1)} %param.29, bf16[32,2048]{1,0:T(8,128)(2,1)S(1)} %copy-done.2, f32[2048]{0:T(1024)S(1)} %copy-done.10, f32[32]{0:T(128)S(1)} %add_rsqrt_fusion.3), kind=kOutput, calls=%fused_computation.5 | convolution fusion | flops 134709248 | bytes 4530304 | tf_op jit(solution)/shard_map/dot_general | solution.py:64
  15.3 0.0 all-reduce.3.cloned.1.call-update
  15.3 0.0 all-gather.2.cloned.1.call-start
  15.3 0.1 copy.41
  15.4 0.1 eq.28
  15.5 0.1 fusion.50
  15.6 0.2 reduce_window_sum.11
  15.8 0.2 select_reduce_fusion
  16.0 0.1 reduce_sum.71
  16.1 0.6 broadcast_multiply_fusion
  16.7 0.1 copy.43
  16.8 0.1 fusion.38
  16.9 19.2 %all-reduce.3.cloned.1.call-done = bf16[32,2048]{1,0:T(8,128)(2,1)} async-done(((bf16[32,2048]{1,0:T(8,128)(2,1)}), bf16[32,2048]{1,0:T(8,128)(2,1)}) %all-reduce.3.cloned.1.call-update) | async-done | bytes 131088 | tf_op jit(solution)/shard_map/psum | solution.py:65
  36.1 1.0 fusion.22
  37.1 1.1 fusion.28
  38.3 0.5 convolution_convert_fusion.1
  38.9 22.2 %all_to_all.17 = bf16[16,16,1024]{2,1,0:T(8,128)(2,1)} all-to-all(bf16[16,16,1024]{2,1,0:T(8,128)(2,1)S(1)} %constant_dynamic-slice_fusion), channel_id=1, replica_groups=mesh['ep'=16,'tp'=2] {'ep'}, dimensions={0} | all-to-all | bytes 1048576 | tf_op jit(solution)/shard_map/all_to_all | solution.py:93
  61.1 0.0 all-gather.2.cloned.1.call-update
  61.1 0.0 reduce-scatter.2.cloned.1.call-start
  61.1 7.5 %all-gather.2.cloned.1.call-done = bf16[1,256,2048]{2,1,0:T(8,128)(2,1)} async-done(((bf16[1,256,1024]{2,1,0:T(8,128)(2,1)}), bf16[1,256,2048]{2,1,0:T(8,128)(2,1)}) %all-gather.2.cloned.1.call-update) | async-done | bytes 1048592 | tf_op jit(solution)/shard_map/all_gather | solution.py:94
  68.6 2.1 %fusion.14 = f32[256,256]{1,0:T(8,128)S(1)} fusion(bf16[1,2048,256]{2,1,0:T(8,128)(2,1)} %param.38, bf16[1,256,2048]{2,1,0:T(8,128)(2,1)} %all-gather.2.cloned.1.call-done), kind=kOutput, calls=%fused_computation.24 | convolution fusion | flops 268435456 | bytes 2359296 | tf_op jit(solution)/shard_map/erd,edf->erf/dot_general | solution.py:97
  70.7 3.8 %fusion = bf16[1,256,2048]{2,1,0:T(8,128)(2,1)} fusion(bf16[1,256,2048]{2,1,0:T(8,128)(2,1)} %param.40, bf16[1,2048,256]{2,1,0:T(8,128)(2,1)} %param.39, bf16[1,256,2048]{2,1,0:T(8,128)(2,1)S(1)} %copy-done.1, f32[256,256]{1,0:T(8,128)S(1)} %fusion.14), kind=kOutput, calls=%fused_computation.3 | convolution fusion | flops 537788416 | bytes 4456448 | tf_op jit(solution)/shard_map/erf,efd->erd/dot_general | solution.py:103
  74.5 0.0 reduce-scatter.2.cloned.1.call-update
  74.6 0.9 mul.225
  75.4 0.8 copy.44
  76.2 8.1 %reduce-scatter.2.cloned.1.call-done = bf16[1,256,1024]{2,1,0:T(8,128)(2,1)} async-done(((bf16[1,256,2048]{2,1,0:T(8,128)(2,1)}), bf16[1,256,1024]{2,1,0:T(8,128)(2,1)}) %reduce-scatter.2.cloned.1.call-update) | async-done | bytes 524304 | tf_op jit(solution)/shard_map/reduce_scatter | solution.py:101
  84.3 1.4 fusion.75
  85.7 1.4 fusion.74
  87.0 1.4 fusion.73
  88.4 1.4 fusion.72
  89.7 1.4 fusion.71
  91.1 1.4 fusion.70
  92.5 1.4 fusion.69
  93.8 1.4 fusion.68
  95.2 1.4 fusion.67
  96.6 1.4 fusion.66
  97.9 1.4 fusion.65
  99.3 1.4 fusion.64
  100.6 1.4 fusion.63
  102.0 1.4 fusion.62
  103.4 1.4 fusion.61
  104.7 1.4 fusion.60
  106.1 6.8 %all-to-all-start.1 = ((bf16[16,1,16,1024]{3,2,1,0:T(8,128)(2,1)}), bf16[16,1,16,1024]{3,2,1,0:T(8,128)(2,1)S(1)}, u32[]{:S(2)}, u32[]{:S(2)}) async-start(bf16[16,1,16,1024]{3,2,1,0:T(8,128)(2,1)} %fusion.60), calls=%async_computation.2 | async-start | bytes 1048576 | tf_op jit(solution)/shard_map/all_to_all | solution.py:110
  112.9 0.0 all-reduce.5.cloned.1.call-start
  113.0 0.7 fusion.39
  113.6 1.5 %fusion.98 = f32[32,256]{1,0:T(8,128)S(1)} fusion(bf16[2048,256]{1,0:T(8,128)(2,1)} %param.41, bf16[32,2048]{1,0:T(8,128)(2,1)S(1)} %get-tuple-element.4, f32[2048]{0:T(1024)S(1)} %copy-done.8, f32[32]{0:T(128)S(1)} %add_rsqrt_fusion.1), kind=kOutput, calls=%fused_computation.144 | convolution fusion | flops 33816576 | bytes 1220736 | tf_op jit(solution)/shard_map/dot_general | solution.py:82
  115.2 3.0 %convolution_convert_fusion.2 = bf16[32,2048]{1,0:T(8,128)(2,1)} fusion(bf16[256,2048]{1,0:T(8,128)(2,1)} %param.43, bf16[2048,256]{1,0:T(8,128)(2,1)} %param.42, f32[32,256]{1,0:T(8,128)S(1)} %fusion.98, bf16[32,2048]{1,0:T(8,128)(2,1)S(1)} %get-tuple-element.4, f32[2048]{0:T(1024)S(1)} %copy-done.8, f32[32]{0:T(128)S(1)} %add_rsqrt_fusion.1), kind=kOutput, calls=%fused_computation.4 | convolution fusion | flops 67485696 | bytes 2400384 | tf_op jit(solution)/shard_map/dot_general | solution.py:87
  118.1 0.0 all-reduce.5.cloned.1.call-update
  118.2 10.2 %all-to-all-done.1 = bf16[16,1,16,1024]{3,2,1,0:T(8,128)(2,1)S(1)} async-done(((bf16[16,1,16,1024]{3,2,1,0:T(8,128)(2,1)}), bf16[16,1,16,1024]{3,2,1,0:T(8,128)(2,1)S(1)}, u32[]{:S(2)}, u32[]{:S(2)}) %all-to-all-start.1) | async-done | bytes 524320 | tf_op jit(solution)/shard_map/all_to_all | solution.py:110
  128.4 0.9 gather_fusion
  129.2 0.2 reshape.138
  129.4 0.4 multiply_reduce_fusion
  129.8 1.9 %all_gather.7 = bf16[32,2048]{1,0:T(8,128)(2,1)S(1)} all-gather(bf16[32,1024]{1,0:T(8,128)(2,1)S(1)} %multiply_reduce_fusion), channel_id=1, replica_groups=mesh['ep'=16,'tp'=2] {'tp'}, dimensions={1}, use_global_device_ids=true | all-gather | bytes 196608 | tf_op jit(solution)/shard_map/all_gather | solution.py:118
  131.7 5.8 %all-reduce.5.cloned.1.call-done = bf16[32,2048]{1,0:T(8,128)(2,1)} async-done(((bf16[32,2048]{1,0:T(8,128)(2,1)}), bf16[32,2048]{1,0:T(8,128)(2,1)}) %all-reduce.5.cloned.1.call-update) | async-done | bytes 131088 | tf_op jit(solution)/shard_map/psum | solution.py:85
  137.5 1.1 multiply_reduce_fusion.1
  138.6 1.7 %fusion.31 = bf16[32,2048]{1,0:T(8,128)(2,1)} fusion(bf16[32,2048]{1,0:T(8,128)(2,1)S(1)} %get-tuple-element.4, bf16[32,2048]{1,0:T(8,128)(2,1)} %all-reduce.5.cloned.1.call-done, bf16[32,2048]{1,0:T(8,128)(2,1)S(1)} %all_gather.7, f32[2048]{0:T(1024)S(1)} %copy-done.11, f32[32]{0:T(128)S(1)} %add_rsqrt_fusion), kind=kLoop, calls=%fused_computation.46 | loop fusion | flops 524288 | bytes 532608 | tf_op jit(solution)/shard_map/convert_element_type | solution.py:120
  (42 shorter events, 0.2 us)
Async XLA Ops:
  7.2 4.8 %copy-start = (bf16[512,2048]{1,0:T(8,128)(2,1)S(1)}, bf16[512,2048]{1,0:T(8,128)(2,1)}, u32[]{:S(2)}) copy-start(bf16[512,2048]{1,0:T(8,128)(2,1)} %param.35) | copy-start | bytes 6291460
  7.2 4.8 %copy-start.2 = (bf16[32,2048]{1,0:T(8,128)(2,1)S(1)}, bf16[32,2048]{1,0:T(8,128)(2,1)}, u32[]{:S(2)}) copy-start(bf16[32,2048]{1,0:T(8,128)(2,1)} %param.22) | copy-start | bytes 393220
  7.2 4.8 %copy-start.10 = (f32[2048]{0:T(1024)S(1)}, f32[2048]{0:T(1024)}, u32[]{:S(2)}) copy-start(f32[2048]{0:T(1024)} %param.25) | copy-start | bytes 24580
  7.2 4.2 %copy-start.3 = (bf16[32,3,512]{2,0,1:T(8,128)(2,1)S(1)}, bf16[32,3,512]{2,0,1:T(8,128)(2,1)}, u32[]{:S(2)}) copy-start(bf16[32,3,512]{2,0,1:T(8,128)(2,1)} %param.24) | copy-start | bytes 294916
  7.2 4.2 %copy-start.15 = (bf16[4,128,128]{2,1,0:T(8,128)(2,1)S(1)}, bf16[4,128,128]{2,1,0:T(8,128)(2,1)}, u32[]{:S(2)}) copy-start(bf16[4,128,128]{2,1,0:T(8,128)(2,1)} %param.33) | copy-start | bytes 393220
  7.2 4.4 %copy-start.16 = (bf16[4,128,128]{2,1,0:T(8,128)(2,1)S(1)}, bf16[4,128,128]{2,1,0:T(8,128)(2,1)}, u32[]{:S(2)}) copy-start(bf16[4,128,128]{2,1,0:T(8,128)(2,1)} %param.32) | copy-start | bytes 393220
  7.2 4.6 %copy-start.14 = (f32[512]{0:T(512)S(1)}, f32[512]{0:T(512)}, u32[]{:S(2)}) copy-start(f32[512]{0:T(512)} %param.34) | copy-start | bytes 6148
  7.2 4.6 %copy-start.9 = (f32[32,512]{1,0:T(8,128)S(1)}, f32[32,512]{1,0:T(8,128)}, u32[]{:S(2)}) copy-start(f32[32,512]{1,0:T(8,128)} %param.23) | copy-start | bytes 196612
  7.3 28.8 %all-reduce.3.cloned.1.call-start = ((), (), s32[]{:S(2)}) async-start(), calls=%async_computation.3 | async-start | bytes 262144 | tf_op jit(solution)/shard_map/psum | solution.py:65
  11.4 3.8 %copy-start.5 = (bf16[32,1,512]{2,0,1:T(8,128)(2,1)}, bf16[32,1,512]{2,0,1:T(8,128)(2,1)S(1)}, u32[]{:S(2)}) copy-start(bf16[32,1,512]{2,0,1:T(8,128)(2,1)S(1)} %fusion.10) | copy-start | bytes 98308
  12.0 3.3 %copy-start.7 = (f32[32,512]{1,0:T(8,128)}, f32[32,512]{1,0:T(8,128)S(1)}, u32[]{:S(2)}) copy-start(f32[32,512]{1,0:T(8,128)S(1)} %fusion.49) | copy-start | bytes 196612
  12.0 3.4 %copy-start.13 = (s32[32,4]{0,1:T(4,128)S(1)}, s32[32,4]{0,1:T(4,128)}, u32[]{:S(2)}) copy-start(s32[32,4]{0,1:T(4,128)} %param.36) | copy-start | bytes 1540
  12.0 25.1 %copy-start.12 = (f32[2048]{0:T(1024)S(1)}, f32[2048]{0:T(1024)}, u32[]{:S(2)}) copy-start(f32[2048]{0:T(1024)} %param.26) | copy-start | bytes 24580
  12.0 26.3 %copy-start.8 = (f32[2048]{0:T(1024)S(1)}, f32[2048]{0:T(1024)}, u32[]{:S(2)}) copy-start(f32[2048]{0:T(1024)} %param.27) | copy-start | bytes 24580
  15.3 53.4 %all-gather.2.cloned.1.call-start = ((), (), s32[]{:S(2)}) async-start(), calls=%async_computation.4 | async-start | bytes 1572864 | tf_op jit(solution)/shard_map/all_gather | solution.py:94
  61.1 23.2 %reduce-scatter.2.cloned.1.call-start = ((), (), s32[]{:S(2)}) async-start(), calls=%async_computation.5 | async-start | bytes 1572864 | tf_op jit(solution)/shard_map/reduce_scatter | solution.py:101
  68.6 2.1 %copy-start.1 = (bf16[1,256,2048]{2,1,0:T(8,128)(2,1)S(1)}, bf16[1,256,2048]{2,1,0:T(8,128)(2,1)}, u32[]{:S(2)}) copy-start(bf16[1,256,2048]{2,1,0:T(8,128)(2,1)} %all-gather.2.cloned.1.call-done) | copy-start | bytes 3145732
  74.5 38.4 %copy-start.4 = (bf16[32,3,512]{2,0,1:T(8,128)(2,1)S(1)}, bf16[32,3,512]{2,0,1:T(8,128)(2,1)}, u32[]{:S(2)}) copy-start(bf16[32,3,512]{2,0,1:T(8,128)(2,1)} %param.24) | copy-start | bytes 294916
  74.5 38.4 %copy-start.6 = (bf16[32,1,512]{2,0,1:T(8,128)(2,1)S(1)}, bf16[32,1,512]{2,0,1:T(8,128)(2,1)}, u32[]{:S(2)}) copy-start(bf16[32,1,512]{2,0,1:T(8,128)(2,1)} %copy-done.5) | copy-start | bytes 98308
  106.1 22.3 %all-to-all-start.1 = ((bf16[16,1,16,1024]{3,2,1,0:T(8,128)(2,1)}), bf16[16,1,16,1024]{3,2,1,0:T(8,128)(2,1)S(1)}, u32[]{:S(2)}, u32[]{:S(2)}) async-start(bf16[16,1,16,1024]{3,2,1,0:T(8,128)(2,1)} %fusion.60), calls=%async_computation.2 | async-start | bytes 1048576 | tf_op jit(solution)/shard_map/all_to_all | solution.py:110
  112.9 24.7 %all-reduce.5.cloned.1.call-start = ((), (), s32[]{:S(2)}) async-start(), calls=%async_computation.6 | async-start | bytes 262144 | tf_op jit(solution)/shard_map/psum | solution.py:85
  128.3 10.2 %copy-start.11 = (f32[2048]{0:T(1024)S(1)}, f32[2048]{0:T(1024)}, u32[]{:S(2)}) copy-start(f32[2048]{0:T(1024)} %param.28) | copy-start | bytes 24580
Sparse Core Ops, SparseCore 0:
  15.4 20.6 all-reduce.2
  61.2 7.3 all-gather.1
  74.7 9.5 reduce-scatter.1
  118.3 19.1 all-reduce.4
